TPU v7x, 32 devices: a whole 2x2x4 slice. The times are simulated.
32 devices in a mesh: rep: 2 (over x), fs: 8 (over z, y), tp: 2 (over core).
Axes of the slice: x: 2, y: 2, z: 4, core: 2. Of those that a mesh axis runs over, the one named last changes fastest.
Arguments:
- tokens: bfloat16 [16, 512, 2048], P(('rep', 'fs')), may hold values from -6 to 6
- gain_mix_pre: float32 [2048], P('fs'), may hold values from 0.1 to 1.9
- gain_mix_post: float32 [2048], P('fs'), may hold values from 0.1 to 1.9
- gain_mlp_pre: float32 [2048], P('fs'), may hold values from 0.1 to 1.9
- gain_mlp_post: float32 [2048], P('fs'), may hold values from 0.1 to 1.9
- x_weight: float32 [2048, 2048], P('fs', 'tp'), may hold values from -0.125 to 0.125
- gate_weight: float32 [2048, 2048], P('fs', 'tp'), may hold values from -0.125 to 0.125
- x_scale: float32 [2048], P('tp'), may hold values from 0.5 to 2
- gate_scale: float32 [2048], P('tp'), may hold values from 0.5 to 2
- conv_weight: float32 [4, 2048], P(None, 'tp'), may hold values from -3 to 3
- recur_map: bfloat16 [2048, 32], P('tp'), may hold values from -1 to 1
- input_map: bfloat16 [2048, 32], P('tp'), may hold values from -1 to 1
- decay_param: float32 [2048], P('tp'), may hold values from 3.9 to 10
- out_weight: float32 [2048, 2048], P('tp', 'fs'), may hold values from -0.125 to 0.125
- out_scale: float32 [2048], P('fs'), may hold values from 0.5 to 2
- up_weight: float32 [2048, 6144], P('fs', 'tp'), may hold values from -0.125 to 0.125
- up_scale: float32 [6144], P('tp'), may hold values from 0.5 to 2
- down_weight: float32 [6144, 2048], P('tp', 'fs'), may hold values from -0.078125 to 0.078125
- down_scale: float32 [2048], P('fs'), may hold values from 0.5 to 2
Outputs:
- layer_out: bfloat16 [16, 512, 2048], P(('rep', 'fs'), 'tp')
All inputs are finite; a program needn't handle non-finite values.
Results may differ from a plain program's by a relative error of at most 0.025.
Values may be sent and summed in bfloat16 or wider, within the bound.
A program may use at most 128 MiB of HBM per device.

v0:
```python
import jax
import jax.numpy as jnp
from jax import lax
from jax.sharding import PartitionSpec as P

BLOCK = 32


EPSILON = 1e-06
DECAY_SCALE = 8.0


def rms_rows(values, gain_vector):
    return (
        values
        * lax.rsqrt(jnp.mean(values * values, axis=-1, keepdims=True) + EPSILON)
        * gain_vector
    )


def link_states(earlier, later):
    return (earlier[0] * later[0], later[0] * earlier[1] + later[1])


def on_device(
    tokens,
    gain_mix_pre,
    gain_mix_post,
    gain_mlp_pre,
    gain_mlp_post,
    x_weight,
    gate_weight,
    x_scale,
    gate_scale,
    conv_weight,
    recur_map,
    input_map,
    decay_param,
    out_weight,
    out_scale,
    up_weight,
    up_scale,
    down_weight,
    down_scale,
):
    resid_in = tokens[0].astype(jnp.float32)
    length = resid_in.shape[0]
    local_width = x_weight.shape[1]
    gathered = (
        lax.all_gather(gain_mix_pre, "fs", axis=0, tiled=True),
        lax.all_gather(gain_mix_post, "fs", axis=0, tiled=True),
        lax.all_gather(gain_mlp_pre, "fs", axis=0, tiled=True),
        lax.all_gather(gain_mlp_post, "fs", axis=0, tiled=True),
        lax.all_gather(out_scale, "fs", axis=0, tiled=True),
        lax.all_gather(down_scale, "fs", axis=0, tiled=True),
    )
    normed = rms_rows(resid_in, gathered[0]).astype(jnp.bfloat16)
    columns = normed
    x_proj = jnp.dot(
        columns,
        lax.all_gather(x_weight.astype(jnp.bfloat16), "fs", axis=0, tiled=True),
        preferred_element_type=jnp.float32,
    )
    gate_proj = jnp.dot(
        columns,
        lax.all_gather(gate_weight.astype(jnp.bfloat16), "fs", axis=0, tiled=True),
        preferred_element_type=jnp.float32,
    )
    out_cols = lax.all_gather(out_weight.astype(jnp.bfloat16), "fs", axis=1, tiled=True)
    down_full = lax.all_gather(down_weight.astype(jnp.bfloat16), "fs", axis=1, tiled=True)
    x_branch = (x_proj * x_scale).astype(jnp.bfloat16)
    gate_branch = (gate_proj * gate_scale).astype(jnp.bfloat16)
    tap_count = conv_weight.shape[0]
    padded = jnp.concatenate(
        [jnp.zeros((tap_count - 1, local_width), jnp.bfloat16), x_branch], axis=0
    )
    conv_sum = conv_weight[0] * padded[0:length].astype(jnp.float32)
    for tap_index in range(1, tap_count):
        conv_sum = conv_sum + conv_weight[tap_index] * padded[
            tap_index : tap_index + length
        ].astype(jnp.float32)
    conv_out = lax.optimization_barrier(conv_sum.astype(jnp.bfloat16))
    blocks = local_width // BLOCK
    conv_blocks = conv_out.reshape(length, blocks, BLOCK)
    recur_logit = jnp.einsum(
        "tnc,ncd->tnd",
        conv_blocks,
        recur_map.reshape(blocks, BLOCK, BLOCK),
        preferred_element_type=jnp.float32,
    ).reshape(length, local_width)
    input_logit = jnp.einsum(
        "tnc,ncd->tnd",
        conv_blocks,
        input_map.reshape(blocks, BLOCK, BLOCK),
        preferred_element_type=jnp.float32,
    ).reshape(length, local_width)
    log_decay = -DECAY_SCALE * jax.nn.sigmoid(recur_logit) * jax.nn.softplus(-decay_param)
    drive = (
        jnp.sqrt(-jnp.expm1(2.0 * log_decay))
        * jax.nn.sigmoid(input_logit)
        * conv_out.astype(jnp.float32)
    )
    _, states = lax.associative_scan(link_states, (jnp.exp(log_decay), drive), axis=0)
    mixed = (states * jax.nn.gelu(gate_branch.astype(jnp.float32))).astype(jnp.bfloat16)
    share_rows = length // lax.axis_size("tp")
    part_rows = mixed
    mix_share = lax.psum_scatter(
        (jnp.dot(part_rows, out_cols, preferred_element_type=jnp.float32) * gathered[4]).astype(
            jnp.bfloat16
        ),
        "tp",
        scatter_dimension=0,
        tiled=True,
    ).astype(jnp.float32)
    offset_row = lax.axis_index("tp") * share_rows
    resid_share = lax.dynamic_slice_in_dim(resid_in, offset_row, share_rows, 0)
    hidden_state = (resid_share + rms_rows(mix_share, gathered[1])).astype(jnp.bfloat16)
    normed_mlp = rms_rows(hidden_state.astype(jnp.float32), gathered[2]).astype(jnp.bfloat16)
    mlp_input = lax.all_gather(normed_mlp, "tp", axis=0, tiled=True)
    columns = mlp_input
    up_proj = jnp.dot(
        columns,
        lax.all_gather(up_weight.astype(jnp.bfloat16), "fs", axis=0, tiled=True),
        preferred_element_type=jnp.float32,
    )
    activated = jnp.square(jax.nn.relu(up_proj * up_scale)).astype(jnp.bfloat16)
    part_rows = activated
    mlp_share = lax.psum_scatter(
        (jnp.dot(part_rows, down_full, preferred_element_type=jnp.float32) * gathered[5]).astype(
            jnp.bfloat16
        ),
        "tp",
        scatter_dimension=0,
        tiled=True,
    ).astype(jnp.float32)
    out_share = (hidden_state.astype(jnp.float32) + rms_rows(mlp_share, gathered[3])).astype(
        jnp.bfloat16
    )
    return out_share[None]


def solution(mesh):
    in_specs = (
        P(("rep", "fs"), None, None),
        P("fs"),
        P("fs"),
        P("fs"),
        P("fs"),
        P("fs", "tp"),
        P("fs", "tp"),
        P("tp"),
        P("tp"),
        P(None, "tp"),
        P("tp", None),
        P("tp", None),
        P("tp"),
        P("tp", "fs"),
        P("fs"),
        P("fs", "tp"),
        P("tp"),
        P("tp", "fs"),
        P("fs"),
    )
    out_specs = P(("rep", "fs"), "tp", None)
    return jax.shard_map(
        on_device, mesh=mesh, in_specs=in_specs, out_specs=out_specs, check_vma=False
    )
```

profile of v0, /device:TPU:0, one launch (start us, length us, event | category | flops | bytes accessed | tf_op | source)
XLA Modules:
  0.0 706.6 jit_solution(5089598831022289540)
XLA Ops:
  6.5 2.2 convert_element_type.85
  12.0 22.6 %all-gather = f32[8,1,256]{2,1,0:T(1,128)S(1)} all-gather(f32[1,1,256]{2,1,0:T(1,128)S(1)} %bitcast.67), channel_id=1, replica_groups=mesh['rep'=2,'fs'=8,'tp'=2] {'fs'}, dimensions={0}, use_global_device_ids=true | all-gather | bytes 9216 | tf_op jit(solution)/shard_map/all_gather | solution.py:50
  36.3 16.9 %all-gather.1 = f32[8,1,256]{2,1,0:T(1,128)} all-gather(f32[1,1,256]{2,1,0:T(1,128)S(1)} %bitcast.68), channel_id=1, replica_groups=mesh['rep'=2,'fs'=8,'tp'=2] {'fs'}, dimensions={0}, use_global_device_ids=true | all-gather | bytes 9216 | tf_op jit(solution)/shard_map/all_gather | solution.py:54
  53.3 31.8 %all-gather.13.cloned.1.call-done = bf16[2048,1024]{1,0:T(8,128)(2,1)} async-done(((bf16[256,1024]{1,0:T(8,128)(2,1)}), bf16[2048,1024]{1,0:T(8,128)(2,1)}) %all-gather.13.cloned.1.call-update) | async-done | bytes 4194320 | tf_op jit(solution)/shard_map/all_gather | solution.py:61
  85.1 4.6 multiply_convert_fusion.4
  99.8 5.2 multiply_exponential_fusion
  105.0 2.8 slice.238
  107.8 2.8 slice.239
  110.7 5.4 slice.237
  116.1 5.5 slice.241
  121.6 3.6 fusion.43
  128.1 3.3 slice.243
  131.4 3.2 slice.247
  134.6 2.7 fusion.44
  195.7 3.3 slice.242
  200.3 5.5 slice.236
  216.3 2.1 pad.71
  219.5 8.6 %pad.73 = f32[512,1024]{1,0:T(8,128)} pad(f32[256,1024]{1,0:T(8,128)} %add.231, f32[]{:T(128)} %constant.19.clone.1), padding=1_0_1x0_0_0 | pad | bytes 3145732 | tf_op jit(solution)/shard_map/pad | solution.py:103
  229.9 4.9 pad.72
  234.9 11.1 %multiply_convert_fusion.2 = bf16[512,2048]{1,0:T(8,128)(2,1)} fusion(bf16[1024,2048]{1,0:T(8,128)(2,1)} %all-gather.17.cloned.1.call-done, f32[2048]{0:T(1024)S(1)} %bitcast.65, f32[512,1024]{1,0:T(8,128)} %pad.72, f32[512,1024]{1,0:T(8,128)} %pad.73, bf16[2048,1024]{1,0:T(8,128)(2,1)} %all-gather.15.cloned.1.call-done, f32[1024]{0:T(1024)S(1)} %copy-done.27, ...), kind=kOutput, calls=%fused_computation.7 | convolution fusion | flops 4308598784 | bytes 16799744 | tf_op jit(solution)/shard_map/dot_general | solution.py:108
  246.0 2.5 convert_element_type.82
  248.5 18.5 %all-gather.2 = f32[8,1,256]{2,1,0:T(1,128)S(1)} all-gather(f32[1,1,256]{2,1,0:T(1,128)S(1)} %bitcast.69), channel_id=1, replica_groups=mesh['rep'=2,'fs'=8,'tp'=2] {'fs'}, dimensions={0}, use_global_device_ids=true | all-gather | bytes 9216 | tf_op jit(solution)/shard_map/all_gather | solution.py:51
  267.0 16.3 %all-gather.3 = f32[8,1,256]{2,1,0:T(1,128)S(1)} all-gather(f32[1,1,256]{2,1,0:T(1,128)S(1)} %bitcast.70), channel_id=1, replica_groups=mesh['rep'=2,'fs'=8,'tp'=2] {'fs'}, dimensions={0}, use_global_device_ids=true | all-gather | bytes 9216 | tf_op jit(solution)/shard_map/all_gather | solution.py:52
  284.9 2.5 fusion.9
  288.7 3.3 convert_element_type.103
  292.1 3.5 convert_element_type.105
  295.7 18.4 %all-gather.4 = f32[8,1,256]{2,1,0:T(1,128)S(1)} all-gather(f32[1,1,256]{2,1,0:T(1,128)S(1)} %bitcast.71), channel_id=1, replica_groups=mesh['rep'=2,'fs'=8,'tp'=2] {'fs'}, dimensions={0}, use_global_device_ids=true | all-gather | bytes 9216 | tf_op jit(solution)/shard_map/all_gather | solution.py:55
  314.0 163.4 %all-gather.21.cloned.1.call-done = bf16[2048,3072]{1,0:T(8,128)(2,1)} async-done(((bf16[256,3072]{1,0:T(8,128)(2,1)}), bf16[2048,3072]{1,0:T(8,128)(2,1)}) %all-gather.21.cloned.1.call-update) | async-done | bytes 12582928 | tf_op jit(solution)/shard_map/all_gather | solution.py:123
  477.5 176.4 %all-gather.23.cloned.1.call-done = bf16[3072,2048]{1,0:T(8,128)(2,1)} async-done(((bf16[3072,256]{1,0:T(8,128)(2,1)}), bf16[3072,2048]{1,0:T(8,128)(2,1)}) %all-gather.23.cloned.1.call-update) | async-done | bytes 12582928 | tf_op jit(solution)/shard_map/all_gather | solution.py:70
  653.8 23.3 %multiply_convert_fusion.1 = bf16[512,2048]{1,0:T(8,128)(2,1)} fusion(bf16[3072,2048]{1,0:T(8,128)(2,1)} %all-gather.23.cloned.1.call-done, f32[2048]{0:T(1024)S(1)} %bitcast.66, bf16[512,2048]{1,0:T(8,128)(2,1)} %all-gather.19.cloned.1.call-done, bf16[2048,3072]{1,0:T(8,128)(2,1)} %all-gather.21.cloned.1.call-done, f32[3072]{0:T(1024)S(1)} %copy-done.25), kind=kOutput, calls=%fused_computation.6 | convolution fusion | flops 12893290496 | bytes 29380608 | tf_op jit(solution)/shard_map/dot_general | solution.py:129
  677.8 17.7 %all-gather.5 = f32[8,1,256]{2,1,0:T(1,128)S(1)} all-gather(f32[1,1,256]{2,1,0:T(1,128)S(1)} %bitcast.72), channel_id=1, replica_groups=mesh['rep'=2,'fs'=8,'tp'=2] {'fs'}, dimensions={0}, use_global_device_ids=true | all-gather | bytes 9216 | tf_op jit(solution)/shard_map/all_gather | solution.py:53
  697.1 2.6 fusion.20
  (186 shorter events, 95.7 us)
Async XLA Ops:
  6.5 2.3 copy-start.4
  6.5 78.6 %all-gather.13.cloned.1.call-start = ((), (), s32[]{:S(2)}) async-start(), calls=%async_computation.2 | async-start | bytes 4718592 | tf_op jit(solution)/shard_map/all_gather | solution.py:61
  8.7 3.3 copy-start.12
  8.8 3.3 copy-start.19
  8.8 25.9 %copy-start = (bf16[1,512,2048]{2,1,0:T(8,128)(2,1)S(1)}, bf16[1,512,2048]{2,1,0:T(8,128)(2,1)}, u32[]{:S(2)}) copy-start(bf16[1,512,2048]{2,1,0:T(8,128)(2,1)} %param.19) | copy-start | bytes 6291460
  8.8 226.0 %all-gather.15.cloned.1.call-start = ((), (), s32[]{:S(2)}) async-start(), calls=%async_computation.3 | async-start | bytes 4718592 | tf_op jit(solution)/shard_map/all_gather | solution.py:66
  9.7 25.4 %copy-start.6 = (bf16[1024,32]{0,1:T(8,128)(2,1)S(1)}, bf16[1024,32]{0,1:T(8,128)(2,1)}, u32[]{:S(2)}) copy-start(bf16[1024,32]{0,1:T(8,128)(2,1)} %param.29) | copy-start | bytes 196612
  9.8 26.3 %copy-start.7 = (bf16[1024,32]{0,1:T(8,128)(2,1)S(1)}, bf16[1024,32]{0,1:T(8,128)(2,1)}, u32[]{:S(2)}) copy-start(bf16[1024,32]{0,1:T(8,128)(2,1)} %param.30) | copy-start | bytes 196612
  9.8 26.5 %copy-start.16 = (f32[1024]{0:T(1024)S(1)}, f32[1024]{0:T(1024)}, u32[]{:S(2)}) copy-start(f32[1024]{0:T(1024)} %param.31) | copy-start | bytes 12292
  9.8 26.5 %copy-start.20 = (f32[256]{0:T(256)S(1)}, f32[256]{0:T(256)}, u32[]{:S(2)}) copy-start(f32[256]{0:T(256)} %param.33) | copy-start | bytes 3076
  9.8 75.3 %copy-start.26 = (f32[1024]{0:T(1024)S(1)}, f32[1024]{0:T(1024)}, u32[]{:S(2)}) copy-start(f32[1024]{0:T(1024)} %param.26) | copy-start | bytes 12292
  9.8 225.0 %all-gather.17.cloned.1.call-start = ((), (), s32[]{:S(2)}) async-start(), calls=%async_computation.4 | async-start | bytes 4718592 | tf_op jit(solution)/shard_map/all_gather | solution.py:69
  12.0 271.4 %reduce-scatter.3.cloned.1.call-start = ((), (), s32[]{:S(2)}) async-start(), calls=%async_computation.5 | async-start | bytes 3145728 | tf_op jit(solution)/shard_map/reduce_scatter | solution.py:107
  34.7 55.0 %copy-start.13 = (f32[8,1,256]{2,1,0:T(1,128)}, f32[8,1,256]{2,1,0:T(1,128)S(1)}, u32[]{:S(2)}) copy-start(f32[8,1,256]{2,1,0:T(1,128)S(1)} %all-gather) | copy-start | bytes 24580
  35.2 54.5 %copy-start.17 = (f32[512]{0:T(512)}, f32[512]{0:T(512)S(1)}, u32[]{:S(2)}) copy-start(f32[512]{0:T(512)S(1)} %add_rsqrt_fusion) | copy-start | bytes 6148
  206.4 7.1 %copy-start.5 = (f32[31,1024]{1,0:T(8,128)S(1)}, f32[31,1024]{1,0:T(8,128)}, u32[]{:S(2)}) copy-start(f32[31,1024]{1,0:T(8,128)} %slice.295) | copy-start | bytes 380932
  206.4 7.1 %copy-start.11 = (f32[1,1024]{1,0:T(1,128)S(1)}, f32[1,1024]{1,0:T(1,128)}, u32[]{:S(2)}) copy-start(f32[1,1024]{1,0:T(1,128)} %slice.305) | copy-start | bytes 12292
  213.8 2.1 copy-start.2
  213.8 2.1 copy-start.3
  229.9 4.9 copy-start.1
  229.9 4.9 copy-start.14
  229.9 4.9 copy-start.15
  229.9 4.9 copy-start.18
  229.9 4.9 copy-start.27
  245.9 68.1 %all-gather.19.cloned.1.call-start = ((), (), s32[]{:S(2)}) async-start(), calls=%async_computation.6 | async-start | bytes 3145728 | tf_op jit(solution)/shard_map/all_gather | solution.py:119
  246.0 2.5 copy-start.21
  246.0 21.0 %copy-start.22 = (f32[256]{0:T(256)S(1)}, f32[256]{0:T(256)}, u32[]{:S(2)}) copy-start(f32[256]{0:T(256)} %param.22) | copy-start | bytes 3076
  288.7 188.8 %all-gather.21.cloned.1.call-start = ((), (), s32[]{:S(2)}) async-start(), calls=%async_computation.7 | async-start | bytes 14155776 | tf_op jit(solution)/shard_map/all_gather | solution.py:123
  292.0 3.6 copy-start.23
  292.1 361.8 %copy-start.25 = (f32[3072]{0:T(1024)S(1)}, f32[3072]{0:T(1024)}, u32[]{:S(2)}) copy-start(f32[3072]{0:T(1024)} %param.35) | copy-start | bytes 36868
  292.1 361.8 %all-gather.23.cloned.1.call-start = ((), (), s32[]{:S(2)}) async-start(), calls=%async_computation.8 | async-start | bytes 14155776 | tf_op jit(solution)/shard_map/all_gather | solution.py:70
  295.6 400.0 %reduce-scatter.5.cloned.1.call-start = ((), (), s32[]{:S(2)}) async-start(), calls=%async_computation.9 | async-start | bytes 3145728 | tf_op jit(solution)/shard_map/reduce_scatter | solution.py:128
  (4 other events, 4.7 us)
Sparse Core Ops, SparseCore 0:
  9.5 75.5 all-gather.12
  87.2 71.3 all-gather.14
  160.6 73.1 all-gather.16
  246.1 8.6 reduce-scatter.2
  288.8 9.2 all-gather.18
  300.1 177.2 all-gather.20
  479.5 174.2 all-gather.22
  677.3 7.9 reduce-scatter.4
where the time goes:
time: 710 us; the launch traced here: 707 us
  waiting for transfers between devices  372 us (52%)
  local copies, waits for them, and re-layouts  110 us (15%)
  blocking collectives  110 us (15%)
  other arithmetic  57 us (8%)
  matrix products  43 us (6%)
  between operations  14.1 us (2%)
    all_gather x1, waiting for transfers between devices, on_device(): lax.all_gather(down_weight.astype(jnp.bfloat16), 'fs', axis=1, tiled=True)  176 us
    all_gather x1, waiting for transfers between devices, on_device(): lax.all_gather(up_weight.astype(jnp.bfloat16), 'fs', axis=0, tiled=True)  163 us
    slice x53, local copies, waits for them, and re-layouts, on_device(): lax.associative_scan(link_states, (jnp.exp(log_decay), drive), axis=0)  86.8 us
    all_gather x1, waiting for transfers between devices, on_device(): lax.all_gather(x_weight.astype(jnp.bfloat16), 'fs', axis=0, tiled=True)  31.8 us
    dot_general x1, matrix products, on_device(): jnp.dot(part_rows, down_full, preferred_element_type=jnp.float32)  23.3 us
    all_gather x1, blocking collectives, on_device(): lax.all_gather(gain_mix_pre, 'fs', axis=0, tiled=True)  22.6 us
    all_gather x1, blocking collectives, on_device(): lax.all_gather(gain_mix_post, 'fs', axis=0, tiled=True)  18.5 us
    all_gather x1, blocking collectives, on_device(): lax.all_gather(down_scale, 'fs', axis=0, tiled=True)  18.4 us
  transfers between devices with their start and end apart: 8, of which 3 were waited for; matrix products, arithmetic and copies ran while one was open for 23% of the time, Pallas kernels for 0%

commit v1 on v0

v1 whole, which is shorter than its diff:
```python
import functools

import jax
import jax.numpy as jnp
from jax import lax
from jax.experimental import pallas as pl
from jax.experimental.pallas import tpu as pltpu
from jax.sharding import PartitionSpec as P

BLOCK = 32
LANES = 128
EPSILON = 1e-06
DECAY_SCALE = 8.0
F32 = jnp.float32
BF16 = jnp.bfloat16


def unit_rows(values):
    return values * lax.rsqrt(jnp.mean(values * values, axis=-1, keepdims=True) + EPSILON)


def shifted(values, distance, fill):
    head = jnp.full((distance, values.shape[1]), fill, values.dtype)
    return jnp.concatenate([head, values[: values.shape[0] - distance]], axis=0)


def mixer_kernel(x_ref, gate_ref, taps_ref, recur_ref, input_ref, rate_ref, mixed_ref):
    length = x_ref.shape[0]
    x_branch = x_ref[...].astype(F32)
    taps = taps_ref.shape[0]
    total = taps_ref[taps - 1 : taps, :] * x_branch
    for tap in range(taps - 1):
        total += taps_ref[tap : tap + 1, :] * shifted(x_branch, taps - 1 - tap, 0.0)
    conv = total.astype(BF16)
    recur = jax.nn.sigmoid(jnp.dot(conv, recur_ref[...], preferred_element_type=F32))
    gate_in = jax.nn.sigmoid(jnp.dot(conv, input_ref[...], preferred_element_type=F32))
    log_decay = recur * rate_ref[0:1, :]
    decay = jnp.exp(log_decay)
    z = -2.0 * log_decay
    series = z * (1.0 - z * (1 / 2) * (1.0 - z * (1 / 3) * (1.0 - z * (1 / 4) * (1.0 - z * (1 / 5)))))
    power = jnp.where(z < 0.1, series, 1.0 - decay * decay)
    state = jnp.sqrt(power) * gate_in * conv.astype(F32)
    distance = 1
    while distance < length:
        state = state + decay * shifted(state, distance, 0.0)
        decay = decay * shifted(decay, distance, 1.0)
        distance *= 2
    mixed_ref[...] = (state * jax.nn.gelu(gate_ref[...].astype(F32))).astype(BF16)


def mixer(branches, taps, recur_dense, input_dense, rate, sequences):
    rows, width = branches.shape[0], branches.shape[1] // 2
    length = rows // sequences
    groups = width // LANES
    return pl.pallas_call(
        mixer_kernel,
        grid=(sequences, groups),
        in_specs=[
            pl.BlockSpec((length, LANES), lambda s, g: (s, g)),
            pl.BlockSpec((length, LANES), lambda s, g: (s, g + groups)),
            pl.BlockSpec((taps.shape[0], LANES), lambda s, g: (0, g)),
            pl.BlockSpec((LANES, LANES), lambda s, g: (g, 0)),
            pl.BlockSpec((LANES, LANES), lambda s, g: (g, 0)),
            pl.BlockSpec((1, LANES), lambda s, g: (0, g)),
        ],
        out_specs=pl.BlockSpec((length, LANES), lambda s, g: (s, g)),
        out_shape=jax.ShapeDtypeStruct((rows, width), BF16),
        cost_estimate=pl.CostEstimate(
            flops=rows * width * 100, bytes_accessed=rows * width * 6, transcendentals=rows * width * 4
        ),
        name="mixer",
    )(branches, branches, taps, recur_dense, input_dense, rate)


def on_device(
    tokens, gain_mix_pre, gain_mix_post, gain_mlp_pre, gain_mlp_post,
    x_weight, gate_weight, x_scale, gate_scale, conv_weight, recur_map, input_map,
    decay_param, out_weight, out_scale, up_weight, up_scale, down_weight, down_scale,
):
    reps = lax.axis_size("rep")
    rep = lax.axis_index("rep")
    team = ("rep", "tp")

    def part(values, axis):
        size = values.shape[axis] // reps
        return lax.dynamic_slice_in_dim(values, rep * size, size, axis)

    length = tokens.shape[1]
    share_rows = length // lax.axis_size("tp")
    offset_row = lax.axis_index("tp") * share_rows
    resid_share = lax.dynamic_slice_in_dim(tokens[0], offset_row, share_rows, 0).astype(F32)
    normed = lax.all_gather(unit_rows(resid_share).astype(BF16), team, axis=0, tiled=True)

    pre = gain_mix_pre[:, None]
    branch_rows = jnp.concatenate(
        [(part(x_weight, 1) * pre).astype(BF16), (part(gate_weight, 1) * pre).astype(BF16)], axis=1
    )
    branch_full = lax.all_gather(branch_rows, "fs", axis=0, tiled=True)
    post = jnp.stack([gain_mix_post, gain_mlp_post])
    post_high = post.astype(BF16)
    post_low = (post - post_high.astype(F32)).astype(BF16)
    pad_rows = jnp.zeros((12, post.shape[1]), BF16)
    out_cols = jnp.concatenate(
        [(part(out_weight, 0) * out_scale).astype(BF16), post_high, post_low, pad_rows], axis=0
    )
    out_all = lax.all_gather(out_cols, "fs", axis=1, tiled=True)
    up_full = lax.all_gather(
        (part(up_weight, 1) * gain_mlp_pre[:, None]).astype(BF16), "fs", axis=0, tiled=True
    )
    down_full = lax.all_gather((part(down_weight, 0) * down_scale).astype(BF16), "fs", axis=1, tiled=True)

    scales = jnp.concatenate([part(x_scale, 0), part(gate_scale, 0)])
    branches = (jnp.dot(normed, branch_full, preferred_element_type=F32) * scales).astype(BF16)
    width = branches.shape[1] // 2

    def dense(block_map):
        rows = lax.broadcasted_iota(jnp.int32, (width, LANES), 0)
        columns = lax.broadcasted_iota(jnp.int32, (width, LANES), 1)
        spread = jnp.tile(part(block_map, 0), (1, LANES // BLOCK))
        return jnp.where(rows % LANES // BLOCK == columns // BLOCK, spread, 0).astype(BF16)

    rate = -DECAY_SCALE * jax.nn.softplus(-part(decay_param, 0))
    mixed = mixer(
        branches, part(conv_weight, 1), dense(recur_map), dense(input_map), rate[None], reps
    )
    out_full = out_all[:width]
    gains = out_all[width : width + 2].astype(F32) + out_all[width + 2 : width + 4].astype(F32)
    mix_share = lax.psum_scatter(
        jnp.dot(mixed, out_full, preferred_element_type=F32).astype(BF16),
        team, scatter_dimension=0, tiled=True,
    ).astype(F32)
    hidden_state = (resid_share + unit_rows(mix_share) * gains[0]).astype(BF16)
    mlp_input = lax.all_gather(
        unit_rows(hidden_state.astype(F32)).astype(BF16), team, axis=0, tiled=True
    )
    up_proj = jnp.dot(mlp_input, up_full, preferred_element_type=F32)
    activated = jnp.square(jax.nn.relu(up_proj * part(up_scale, 0))).astype(BF16)
    mlp_share = lax.psum_scatter(
        jnp.dot(activated, down_full, preferred_element_type=F32).astype(BF16),
        team, scatter_dimension=0, tiled=True,
    ).astype(F32)
    return (hidden_state.astype(F32) + unit_rows(mlp_share) * gains[1]).astype(BF16)[None]


def solution(mesh):
    in_specs = (
        P(("rep", "fs"), None, None),
        P("fs"), P("fs"), P("fs"), P("fs"),
        P("fs", "tp"), P("fs", "tp"),
        P("tp"), P("tp"),
        P(None, "tp"), P("tp", None), P("tp", None), P("tp"),
        P("tp", "fs"), P("fs"),
        P("fs", "tp"), P("tp"),
        P("tp", "fs"), P("fs"),
    )
    out_specs = P(("rep", "fs"), "tp", None)
    return jax.shard_map(
        on_device, mesh=mesh, in_specs=in_specs, out_specs=out_specs, check_vma=False
    )
```

time: 710 us -> 535 us (0.75)
  blocking collectives: 110 us -> 0 us
  local copies, waits for them, and re-layouts: 110 us -> 3.08 us
  waiting for transfers between devices: 372 us -> 450 us
  other arithmetic: 57 us -> 21.5 us
  Pallas kernels: 0 us -> 9.56 us
  matrix products: 43 us -> 35.4 us
    all_gather x6 -> x0, blocking collectives: 110 us -> none  [the longest x1 22.6 us: on_device(): lax.all_gather(gain_mix_pre, 'fs', axis=0, tiled=True)]
    slice x54 -> x1, local copies, waits for them, and re-layouts: 86.8 us -> 0.01 us  [on_device(): gains[1]]
    reduce_scatter x2, waiting for transfers between devices: 0.01 us -> 80.7 us  [the longest x1 44.8 us: on_device(): lax.psum_scatter(jnp.dot(activated, down_full, preferred_element_type=F32...]
    pad x16 -> x0, local copies, waits for them, and re-layouts: 16.1 us -> none  [on_device(): lax.associative_scan(link_states, (jnp.exp(log_decay), drive), axis=0)]
    mul x8 -> x1, other arithmetic: 14.6 us -> 0.69 us  [on_device(): rate = -DECAY_SCALE * jax.nn.softplus(-part(decay_param, 0))]
    pallas_call x0 -> x1, Pallas kernels: none -> 9.56 us  [mixer(): pl.pallas_call(mixer_kernel, grid=(sequences, groups), in_specs=[pl.Block...]
    convert_element_type x8, other arithmetic: 16.6 us -> 7.89 us  [the longest x1 3.01 us: on_device(): (part(down_weight, 0) * down_scale).astype(BF16)]
    add x17 -> x1, other arithmetic: 8.92 us -> 0.85 us  [on_device(): out_all[width:width + 2].astype(F32)]
  transfers between devices with their start and end apart: 8 -> 8, of which waited for: 3 -> 8; matrix products, arithmetic and copies ran while one was open for 23% -> 4% of each run, Pallas kernels for 0% -> 2%
where the time goes in v1:
time: 535 us; the launch traced here: 534 us
  waiting for transfers between devices  450 us (84%)
  matrix products  35.4 us (7%)
  other arithmetic  21.5 us (4%)
  between operations  13.8 us (3%)
  Pallas kernels  9.56 us (2%)
    all_gather x1, waiting for transfers between devices, on_device(): lax.all_gather((part(down_weight, 0) * down_scale).astype(BF16), 'fs', ax...  99.6 us
    all_gather x1, waiting for transfers between devices, on_device(): lax.all_gather((part(up_weight, 1) * gain_mlp_pre[:, None]).astype(BF16),...  95.8 us
    all_gather x1, waiting for transfers between devices, on_device(): branch_full = lax.all_gather(branch_rows, 'fs', axis=0, tiled=True)  75 us
    reduce_scatter x1, waiting for transfers between devices, on_device(): lax.psum_scatter(jnp.dot(activated, down_full, preferred_element_type=F32...  44.8 us
    reduce_scatter x1, waiting for transfers between devices, on_device(): lax.psum_scatter(jnp.dot(mixed, out_full, preferred_element_type=F32).ast...  36 us
    all_gather x1, waiting for transfers between devices, on_device(): lax.all_gather(unit_rows(hidden_state.astype(F32)).astype(BF16), team, ax...  34.2 us
    all_gather x1, waiting for transfers between devices, on_device(): out_all = lax.all_gather(out_cols, 'fs', axis=1, tiled=True)  32.9 us
    all_gather x1, waiting for transfers between devices, on_device(): lax.all_gather(unit_rows(resid_share).astype(BF16), team, axis=0, tiled=T...  32.1 us
  transfers between devices with their start and end apart: 8, of which 8 were waited for; matrix products, arithmetic and copies ran while one was open for 4% of the time, Pallas kernels for 2%

profile of v1, /device:TPU:0, one launch (start us, length us, event | category | flops | bytes accessed | tf_op | source)
XLA Modules:
  0.0 534.1 jit_solution(14196632873459750633)
XLA Ops:
  6.6 1.7 fusion.7
  8.3 2.4 fusion.8
  10.9 0.1 multiply_convert_fusion.6
  11.0 0.9 pad_maximum_fusion
  12.2 0.9 maximum_maximum_fusion
  13.4 0.1 copy.22
  13.5 0.1 copy.23
  13.7 0.7 fusion.18
  14.4 0.6 constant_dynamic-slice_fusion.2.taps_ref
  15.0 1.0 broadcast_select_fusion
  16.0 32.1 %all-gather.7.cloned.1.call-done = bf16[1024,2048]{1,0:T(8,128)(2,1)} async-done(((bf16[256,2048]{1,0:T(8,128)(2,1)}), bf16[1024,2048]{1,0:T(8,128)(2,1)}) %all-gather.7.cloned.1.call-update) | async-done | bytes 4194320 | tf_op jit(solution)/shard_map/all_gather | solution.py:92
  48.1 75.0 %all-gather.9.cloned.1.call-done = bf16[2048,1024]{1,0:T(8,128)(2,1)} async-done(((bf16[256,1024]{1,0:T(8,128)(2,1)}), bf16[2048,1024]{1,0:T(8,128)(2,1)}) %all-gather.9.cloned.1.call-update) | async-done | bytes 4194320 | tf_op jit(solution)/shard_map/all_gather | solution.py:98
  123.0 9.3 %multiply_convert_fusion.1.x_ref.gate_ref = bf16[1024,1024]{1,0:T(8,128)(2,1)} fusion(bf16[1024,2048]{1,0:T(8,128)(2,1)} %all-gather.7.cloned.1.call-done, bf16[2048,1024]{1,0:T(8,128)(2,1)} %all-gather.9.cloned.1.call-done, f32[1024]{0:T(1024)S(1)} %pad_maximum_fusion.1), kind=kOutput, calls=%fused_computation.1 | convolution fusion | flops 4297064448 | bytes 10489856 | tf_op jit(solution)/shard_map/dot_general | solution.py:113
  132.3 9.6 %mixer.1 = bf16[1024,512]{1,0:T(8,128)(2,1)} custom-call(bf16[1024,1024]{1,0:T(8,128)(2,1)} %multiply_convert_fusion.1.x_ref.gate_ref, bf16[1024,1024]{1,0:T(8,128)(2,1)} %multiply_convert_fusion.1.x_ref.gate_ref, f32[4,512]{1,0:T(4,128)} %constant_dynamic-slice_fusion.2.taps_ref, bf16[512,128]{1,0:T(8,128)(2,1)} %get-tuple-element.10.recur_ref, ...), custom_call_target="tpu_custom_call" | custom-call | flops 52428800 | bytes 3145728 | tf_op jit(solution)/shard_map/mixer/pallas_call | solution.py:55
  141.9 32.9 %all-gather.11.cloned.1.call-done = bf16[528,2048]{1,0:T(8,128)(2,1)} async-done(((bf16[528,256]{1,0:T(8,128)(2,1)}), bf16[528,2048]{1,0:T(8,128)(2,1)}) %all-gather.11.cloned.1.call-update) | async-done | bytes 2162704 | tf_op jit(solution)/shard_map/all_gather | solution.py:106
  174.8 6.2 %convolution_convert_fusion.1 = bf16[1024,2048]{1,0:T(8,128)(2,1)} fusion(bf16[1024,512]{1,0:T(8,128)(2,1)} %mixer.1, bf16[528,2048]{1,0:T(8,128)(2,1)} %all-gather.11.cloned.1.call-done), kind=kOutput, calls=%fused_computation.3 | convolution fusion | flops 2149580800 | bytes 7340032 | tf_op jit(solution)/shard_map/dot_general | solution.py:129
  181.1 1.8 copy-done.2
  182.9 1.0 multiply_convert_fusion.3
  184.0 3.0 multiply_convert_fusion.2
  187.1 0.8 convert_add_fusion.2
  187.9 36.0 %reduce-scatter.3.cloned.1.call-done = bf16[256,2048]{1,0:T(8,128)(2,1)} async-done(((bf16[1024,2048]{1,0:T(8,128)(2,1)}), bf16[256,2048]{1,0:T(8,128)(2,1)}) %reduce-scatter.3.cloned.1.call-update) | async-done | bytes 1048592 | tf_op jit(solution)/shard_map/reduce_scatter | solution.py:128
  223.9 1.5 fusion
  225.4 1.9 fusion.4
  227.4 1.2 fusion.5
  228.6 0.2 reduce-scatter.5.cloned.1.call-start
  228.9 95.8 %all-gather.15.cloned.1.call-done = bf16[2048,1536]{1,0:T(8,128)(2,1)} async-done(((bf16[256,1536]{1,0:T(8,128)(2,1)}), bf16[2048,1536]{1,0:T(8,128)(2,1)}) %all-gather.15.cloned.1.call-update) | async-done | bytes 6291472 | tf_op jit(solution)/shard_map/all_gather | solution.py:107
  324.7 99.6 %all-gather.17.cloned.1.call-done = bf16[1536,2048]{1,0:T(8,128)(2,1)} async-done(((bf16[1536,256]{1,0:T(8,128)(2,1)}), bf16[1536,2048]{1,0:T(8,128)(2,1)}) %all-gather.17.cloned.1.call-update) | async-done | bytes 6291472 | tf_op jit(solution)/shard_map/all_gather | solution.py:110
  424.3 34.2 %all-gather.13.cloned.1.call-done = bf16[1024,2048]{1,0:T(8,128)(2,1)} async-done(((bf16[256,2048]{1,0:T(8,128)(2,1)}), bf16[1024,2048]{1,0:T(8,128)(2,1)}) %all-gather.13.cloned.1.call-update) | async-done | bytes 4194320 | tf_op jit(solution)/shard_map/all_gather | solution.py:133
  458.5 19.9 %convolution_convert_fusion = bf16[1024,2048]{1,0:T(8,128)(2,1)} fusion(bf16[1536,2048]{1,0:T(8,128)(2,1)} %all-gather.17.cloned.1.call-done, bf16[1024,2048]{1,0:T(8,128)(2,1)} %all-gather.13.cloned.1.call-done, bf16[2048,1536]{1,0:T(8,128)(2,1)} %all-gather.15.cloned.1.call-done, f32[1536]{0:T(1024)S(1)} %dynamic_slice.50), kind=kOutput, calls=%fused_computation.2 | convolution fusion | flops 12893290496 | bytes 20977664 | tf_op jit(solution)/shard_map/dot_general | solution.py:139
  478.4 44.8 %reduce-scatter.5.cloned.1.call-done = bf16[256,2048]{1,0:T(8,128)(2,1)} async-done(((bf16[1024,2048]{1,0:T(8,128)(2,1)}), bf16[256,2048]{1,0:T(8,128)(2,1)}) %reduce-scatter.5.cloned.1.call-update) | async-done | bytes 1048592 | tf_op jit(solution)/shard_map/reduce_scatter | solution.py:138
  523.1 1.5 fusion.2
  524.6 2.6 fusion.11
  (71 shorter events, 1.0 us)
Async XLA Ops:
  6.5 7.8 %copy-start = (f32[4,1024]{1,0:T(4,128)S(1)}, f32[4,1024]{1,0:T(4,128)}, u32[]{:S(2)}) copy-start(f32[4,1024]{1,0:T(4,128)} %param.28) | copy-start | bytes 49156
  6.5 4.3 copy-start.11
  6.5 4.3 copy-start.3
  6.5 4.3 copy-start.4
  6.5 41.5 %all-gather.7.cloned.1.call-start = ((), (), s32[]{:S(2)}) async-start(), calls=%async_computation.2 | async-start | bytes 5242880 | tf_op jit(solution)/shard_map/all_gather | solution.py:92
  10.7 1.4 copy-start.9
  10.7 1.4 copy-start.10
  10.7 1.4 copy-start.5
  10.7 1.5 copy-start.12
  10.7 112.3 %all-gather.9.cloned.1.call-start = ((), (), s32[]{:S(2)}) async-start(), calls=%async_computation.3 | async-start | bytes 4718592 | tf_op jit(solution)/shard_map/all_gather | solution.py:98
  10.8 2.3 copy-start.15
  10.8 2.4 copy-start.16
  10.8 2.5 copy-start.6
  10.9 2.5 copy-start.7
  11.0 2.7 copy-start.17
  12.0 162.8 %all-gather.11.cloned.1.call-start = ((), (), s32[]{:S(2)}) async-start(), calls=%async_computation.4 | async-start | bytes 2433024 | tf_op jit(solution)/shard_map/all_gather | solution.py:106
  13.1 210.8 %reduce-scatter.3.cloned.1.call-start = ((), (), s32[]{:S(2)}) async-start(), calls=%async_computation.5 | async-start | bytes 5242880 | tf_op jit(solution)/shard_map/reduce_scatter | solution.py:128
  181.0 1.9 copy-start.2
  181.0 1.9 copy-start.13
  181.0 3.0 copy-start.14
  181.0 143.7 %all-gather.15.cloned.1.call-start = ((), (), s32[]{:S(2)}) async-start(), calls=%async_computation.7 | async-start | bytes 7077888 | tf_op jit(solution)/shard_map/all_gather | solution.py:107
  183.9 41.5 %copy-start.1 = (bf16[1,512,2048]{2,1,0:T(8,128)(2,1)S(1)}, bf16[1,512,2048]{2,1,0:T(8,128)(2,1)}, u32[]{:S(2)}) copy-start(bf16[1,512,2048]{2,1,0:T(8,128)(2,1)} %param.19) | copy-start | bytes 6291460
  183.9 240.3 %all-gather.17.cloned.1.call-start = ((), (), s32[]{:S(2)}) async-start(), calls=%async_computation.8 | async-start | bytes 7077888 | tf_op jit(solution)/shard_map/all_gather | solution.py:110
  187.0 271.5 %all-gather.13.cloned.1.call-start = ((), (), s32[]{:S(2)}) async-start(), calls=%async_computation.6 | async-start | bytes 5242880 | tf_op jit(solution)/shard_map/all_gather | solution.py:133
  227.3 1.5 copy-start.8
  228.6 294.5 %reduce-scatter.5.cloned.1.call-start = ((), (), s32[]{:S(2)}) async-start(), calls=%async_computation.9 | async-start | bytes 5242880 | tf_op jit(solution)/shard_map/reduce_scatter | solution.py:138
Sparse Core Ops, SparseCore 0:
  10.9 37.1 all-gather.6
  50.2 72.7 all-gather.8
  125.1 49.6 all-gather.10
  181.1 42.7 reduce-scatter.2
  225.9 98.6 all-gather.14
  326.6 97.6 all-gather.16
  425.8 32.6 all-gather.12
  478.5 44.5 reduce-scatter.4

commit v2 on v1

--- a/solution.py
+++ b/solution.py
@@ -72,6 +72,210 @@
     )(branches, branches, taps, recur_dense, input_dense, rate)
 
 
+MESH_IDS = pl.DeviceIdType.MESH
+
+
+def greet(peers):
+    barrier = pltpu.get_barrier_semaphore()
+    for peer in peers:
+        pl.semaphore_signal(barrier, inc=1, device_id=peer, device_id_type=MESH_IDS)
+    pl.semaphore_wait(barrier, len(peers))
+
+
+def push(source, target, sent, landed, peer):
+    return pltpu.make_async_remote_copy(
+        src_ref=source, dst_ref=target, send_sem=sent, recv_sem=landed,
+        device_id=peer, device_id_type=MESH_IDS,
+    )
+
+
+def others(axis, count):
+    me = lax.axis_index(axis)
+    return [lax.rem(me + step, count) for step in range(1, count)]
+
+
+def row_block(ref, index, rows):
+    return ref.at[pl.ds(pl.multiple_of(index * rows, rows), rows)]
+
+
+def team_gather_kernel(reps, tps, x_ref, out_ref, own_sem, sent, landed):
+    rep, core = lax.axis_index("rep"), lax.axis_index("tp")
+    rows = x_ref.shape[0]
+    rep_peers, tp_peers = others("rep", reps), others("tp", tps)
+    greet([{"rep": peer} for peer in rep_peers] + [{"tp": peer} for peer in tp_peers])
+    mine = row_block(out_ref, rep * tps + core, rows)
+    flights = []
+    for step, peer in enumerate(rep_peers):
+        copy = push(x_ref, mine, sent.at[step + 1, 0], landed.at[step + 1, 0], {"rep": peer})
+        copy.start()
+        flights.append(copy)
+    own = pltpu.make_async_copy(x_ref, mine, own_sem)
+    own.start()
+    local = []
+    for slot, peer in enumerate(tp_peers):
+        copy = push(x_ref, mine, sent.at[0, slot + 1], landed.at[0, slot + 1], {"tp": peer})
+        copy.start()
+        local.append(copy)
+    for step in range(1, reps):
+        flights[step - 1].wait_recv()
+        source = lax.rem(rep + reps - step, reps)
+        block = row_block(out_ref, source * tps + core, rows)
+        for slot, peer in enumerate(tp_peers):
+            copy = push(block, block, sent.at[step, slot + 1], landed.at[step, slot + 1], {"tp": peer})
+            copy.start()
+            local.append(copy)
+    for copy in flights:
+        copy.wait_send()
+    for copy in local:
+        copy.wait()
+    own.wait()
+
+
+def team_gather(values):
+    reps, tps = lax.axis_size("rep"), lax.axis_size("tp")
+    rows, width = values.shape
+    return pl.pallas_call(
+        functools.partial(team_gather_kernel, reps, tps),
+        out_shape=jax.ShapeDtypeStruct((rows * reps * tps, width), values.dtype),
+        in_specs=[pl.BlockSpec(memory_space=pltpu.VMEM)],
+        out_specs=pl.BlockSpec(memory_space=pltpu.VMEM),
+        scratch_shapes=[
+            pltpu.SemaphoreType.DMA,
+            pltpu.SemaphoreType.DMA((reps, tps)),
+            pltpu.SemaphoreType.DMA((reps, tps)),
+        ],
+        compiler_params=pltpu.CompilerParams(collective_id=0, has_side_effects=True),
+        cost_estimate=pl.CostEstimate(flops=0, bytes_accessed=80_000_000, transcendentals=0),
+        name="team_gather",
+    )(values)
+
+
+def team_sum_kernel(reps, tps, part_ref, out_ref, got, stage, last, sent, landed, sent_far, landed_far):
+    rep, core = lax.axis_index("rep"), lax.axis_index("tp")
+    rows = out_ref.shape[0]
+    step_rows = 16
+    rep_peers, tp_peers = others("rep", reps), others("tp", tps)
+    greet([{"rep": peer} for peer in rep_peers] + [{"tp": peer} for peer in tp_peers])
+    near = []
+    for slot, peer in enumerate(tp_peers):
+        for group in range(reps):
+            copy = push(
+                row_block(part_ref, group * tps + peer, rows), got.at[slot, group],
+                sent.at[slot, group], landed.at[slot, group], {"tp": peer},
+            )
+            copy.start()
+            near.append(copy)
+    for copy in near:
+        copy.wait()
+
+    def total(group, start):
+        base = pl.multiple_of((group * tps + core) * rows + start, step_rows)
+        value = part_ref[pl.ds(base, step_rows)].astype(F32)
+        for slot in range(tps - 1):
+            value += got[slot, group, pl.ds(start, step_rows)].astype(F32)
+        return value
+
+    far = []
+    for step, peer in enumerate(rep_peers):
+
+        def fill(index, carry):
+            start = pl.multiple_of(index * step_rows, step_rows)
+            stage[step, pl.ds(start, step_rows)] = total(peer, start).astype(BF16)
+            return carry
+
+        lax.fori_loop(0, rows // step_rows, fill, 0)
+        copy = push(stage.at[step], last.at[step], sent_far.at[step], landed_far.at[step], {"rep": peer})
+        copy.start()
+        far.append(copy)
+    for copy in far:
+        copy.wait()
+
+    def finish(index, carry):
+        start = pl.multiple_of(index * step_rows, step_rows)
+        value = total(rep, start)
+        for step in range(reps - 1):
+            value += last[step, pl.ds(start, step_rows)].astype(F32)
+        out_ref[pl.ds(start, step_rows)] = value
+        return carry
+
+    lax.fori_loop(0, rows // step_rows, finish, 0)
+
+
+def team_sum(parts):
+    reps, tps = lax.axis_size("rep"), lax.axis_size("tp")
+    rows, width = parts.shape[0] // (reps * tps), parts.shape[1]
+    return pl.pallas_call(
+        functools.partial(team_sum_kernel, reps, tps),
+        out_shape=jax.ShapeDtypeStruct((rows, width), F32),
+        in_specs=[pl.BlockSpec(memory_space=pltpu.VMEM)],
+        out_specs=pl.BlockSpec(memory_space=pltpu.VMEM),
+        scratch_shapes=[
+            pltpu.VMEM((tps - 1, reps, rows, width), BF16),
+            pltpu.VMEM((reps - 1, rows, width), BF16),
+            pltpu.VMEM((reps - 1, rows, width), BF16),
+            pltpu.SemaphoreType.DMA((tps - 1, reps)),
+            pltpu.SemaphoreType.DMA((tps - 1, reps)),
+            pltpu.SemaphoreType.DMA((reps - 1,)),
+            pltpu.SemaphoreType.DMA((reps - 1,)),
+        ],
+        compiler_params=pltpu.CompilerParams(collective_id=1, has_side_effects=True),
+        cost_estimate=pl.CostEstimate(flops=0, bytes_accessed=80_000_000, transcendentals=0),
+        name="team_sum",
+    )(parts)
+
+
+def shard_gather_kernel(shards, x_ref, out_ref, own_sem, sent, landed, sent_pass, landed_pass):
+    me = lax.axis_index("fs")
+    rows = x_ref.shape[0]
+    pairs = shards // 2
+    pair, parity = me // 2, lax.rem(me, 2)
+    partner = {"fs": pair * 2 + 1 - parity}
+    peers = [{"fs": lax.rem(pair + step, pairs) * 2 + parity} for step in range(1, pairs)]
+    greet([partner] + peers)
+    mine = row_block(out_ref, me, rows)
+    passed = [push(x_ref, mine, sent_pass.at[0], landed_pass.at[0], partner)]
+    passed[0].start()
+    direct = []
+    for step, peer in enumerate(peers):
+        copy = push(x_ref, mine, sent.at[step], landed.at[step], peer)
+        copy.start()
+        direct.append(copy)
+    own = pltpu.make_async_copy(x_ref, mine, own_sem)
+    own.start()
+    for step in range(1, pairs):
+        direct[step - 1].wait_recv()
+        block = row_block(out_ref, lax.rem(pair + pairs - step, pairs) * 2 + parity, rows)
+        copy = push(block, block, sent_pass.at[step], landed_pass.at[step], partner)
+        copy.start()
+        passed.append(copy)
+    for copy in direct:
+        copy.wait_send()
+    for copy in passed:
+        copy.wait()
+    own.wait()
+
+
+def shard_gather(values, collective_id):
+    shards = lax.axis_size("fs")
+    rows, width = values.shape
+    return pl.pallas_call(
+        functools.partial(shard_gather_kernel, shards),
+        out_shape=jax.ShapeDtypeStruct((rows * shards, width), values.dtype),
+        in_specs=[pl.BlockSpec(memory_space=pltpu.VMEM)],
+        out_specs=pl.BlockSpec(memory_space=pltpu.VMEM),
+        scratch_shapes=[
+            pltpu.SemaphoreType.DMA,
+            pltpu.SemaphoreType.DMA((shards // 2,)),
+            pltpu.SemaphoreType.DMA((shards // 2,)),
+            pltpu.SemaphoreType.DMA((shards // 2,)),
+            pltpu.SemaphoreType.DMA((shards // 2,)),
+        ],
+        compiler_params=pltpu.CompilerParams(collective_id=collective_id, has_side_effects=True),
+        cost_estimate=pl.CostEstimate(flops=0, bytes_accessed=200_000_000, transcendentals=0),
+        name="shard_gather",
+    )(values)
+
+
 def on_device(
     tokens, gain_mix_pre, gain_mix_post, gain_mlp_pre, gain_mlp_post,
     x_weight, gate_weight, x_scale, gate_scale, conv_weight, recur_map, input_map,
@@ -79,7 +283,6 @@
 ):
     reps = lax.axis_size("rep")
     rep = lax.axis_index("rep")
-    team = ("rep", "tp")
 
     def part(values, axis):
         size = values.shape[axis] // reps
@@ -89,12 +292,13 @@
     share_rows = length // lax.axis_size("tp")
     offset_row = lax.axis_index("tp") * share_rows
     resid_share = lax.dynamic_slice_in_dim(tokens[0], offset_row, share_rows, 0).astype(F32)
-    normed = lax.all_gather(unit_rows(resid_share).astype(BF16), team, axis=0, tiled=True)
+    normed_share = unit_rows(resid_share).astype(BF16)
 
     pre = gain_mix_pre[:, None]
     branch_rows = jnp.concatenate(
         [(part(x_weight, 1) * pre).astype(BF16), (part(gate_weight, 1) * pre).astype(BF16)], axis=1
     )
+    branch_rows, out_weight = lax.optimization_barrier((branch_rows, out_weight))
     branch_full = lax.all_gather(branch_rows, "fs", axis=0, tiled=True)
     post = jnp.stack([gain_mix_post, gain_mlp_post])
     post_high = post.astype(BF16)
@@ -103,11 +307,14 @@
     out_cols = jnp.concatenate(
         [(part(out_weight, 0) * out_scale).astype(BF16), post_high, post_low, pad_rows], axis=0
     )
+    out_cols, down_weight = lax.optimization_barrier((out_cols, down_weight))
     out_all = lax.all_gather(out_cols, "fs", axis=1, tiled=True)
-    up_full = lax.all_gather(
-        (part(up_weight, 1) * gain_mlp_pre[:, None]).astype(BF16), "fs", axis=0, tiled=True
-    )
     down_full = lax.all_gather((part(down_weight, 0) * down_scale).astype(BF16), "fs", axis=1, tiled=True)
+    up_rows = (part(up_weight, 1) * gain_mlp_pre[:, None]).astype(BF16)
+    normed = team_gather(normed_share)
+    normed, up_rows = lax.optimization_barrier((normed, up_rows))
+    up_full = shard_gather(up_rows, 2)
+    normed, up_full = lax.optimization_barrier((normed, up_full))
 
     scales = jnp.concatenate([part(x_scale, 0), part(gate_scale, 0)])
     branches = (jnp.dot(normed, branch_full, preferred_element_type=F32) * scales).astype(BF16)
@@ -125,20 +332,12 @@
     )
     out_full = out_all[:width]
     gains = out_all[width : width + 2].astype(F32) + out_all[width + 2 : width + 4].astype(F32)
-    mix_share = lax.psum_scatter(
-        jnp.dot(mixed, out_full, preferred_element_type=F32).astype(BF16),
-        team, scatter_dimension=0, tiled=True,
-    ).astype(F32)
+    mix_share = team_sum(jnp.dot(mixed, out_full, preferred_element_type=F32).astype(BF16))
     hidden_state = (resid_share + unit_rows(mix_share) * gains[0]).astype(BF16)
-    mlp_input = lax.all_gather(
-        unit_rows(hidden_state.astype(F32)).astype(BF16), team, axis=0, tiled=True
-    )
+    mlp_input = team_gather(unit_rows(hidden_state.astype(F32)).astype(BF16))
     up_proj = jnp.dot(mlp_input, up_full, preferred_element_type=F32)
     activated = jnp.square(jax.nn.relu(up_proj * part(up_scale, 0))).astype(BF16)
-    mlp_share = lax.psum_scatter(
-        jnp.dot(activated, down_full, preferred_element_type=F32).astype(BF16),
-        team, scatter_dimension=0, tiled=True,
-    ).astype(F32)
+    mlp_share = team_sum(jnp.dot(activated, down_full, preferred_element_type=F32).astype(BF16))
     return (hidden_state.astype(F32) + unit_rows(mlp_share) * gains[1]).astype(BF16)[None]
 
 

time: 535 us -> 380 us (0.71)
  waiting for transfers between devices: 450 us -> 63.5 us
  Pallas kernels: 9.56 us -> 244 us
    pallas_call x0 -> x5, Pallas kernels: none -> 234 us  [the longest x1 103 us: shard_gather(): pl.pallas_call(functools.partial(shard_gather_kernel, shards), out_shape=...]
    all_gather x3 -> x0, waiting for transfers between devices: 162 us -> none  [the longest x1 95.8 us: on_device(): lax.all_gather((part(up_weight, 1) * gain_mlp_pre[:, None]).astype(BF16),...]
    reduce_scatter x2 -> x0, waiting for transfers between devices: 80.7 us -> none  [the longest x1 44.8 us: on_device(): lax.psum_scatter(jnp.dot(activated, down_full, preferred_element_type=F32...]
    all_gather x1, waiting for transfers between devices: 99.6 us -> 21.2 us  [on_device(): lax.all_gather((part(down_weight, 0) * down_scale).astype(BF16), 'fs', ax...]
    all_gather x1, waiting for transfers between devices: 75 us -> 41.6 us  [on_device(): branch_full = lax.all_gather(branch_rows, 'fs', axis=0, tiled=True)]
    all_gather x1, waiting for transfers between devices: 32.9 us -> 0.01 us  [on_device(): out_all = lax.all_gather(out_cols, 'fs', axis=1, tiled=True)]
  transfers between devices with their start and end apart: 8 -> 3, of which waited for: 8 -> 2; matrix products, arithmetic and copies ran while one was open for 4% -> 8% of each run, Pallas kernels for 2% -> 55%
where the time goes in v2:
time: 380 us; the launch traced here: 379 us
  Pallas kernels  244 us (64%)
  waiting for transfers between devices  63.5 us (17%)
  matrix products  35.4 us (9%)
  other arithmetic  20.8 us (5%)
  between operations  13.4 us (4%)
    pallas_call x1, Pallas kernels, shard_gather(): pl.pallas_call(functools.partial(shard_gather_kernel, shards), out_shape=...  103 us
    pallas_call x2, Pallas kernels, team_sum(): pl.pallas_call(functools.partial(team_sum_kernel, reps, tps), out_shape=j...  67.9 us
    pallas_call x2, Pallas kernels, team_gather(): pl.pallas_call(functools.partial(team_gather_kernel, reps, tps), out_shap...  63.2 us
    all_gather x1, waiting for transfers between devices, on_device(): branch_full = lax.all_gather(branch_rows, 'fs', axis=0, tiled=True)  41.6 us
    all_gather x1, waiting for transfers between devices, on_device(): lax.all_gather((part(down_weight, 0) * down_scale).astype(BF16), 'fs', ax...  21.2 us
    dot_general x1, matrix products, on_device(): jnp.dot(activated, down_full, preferred_element_type=F32).astype(BF16)  19.9 us
    pallas_call x1, Pallas kernels, mixer(): pl.pallas_call(mixer_kernel, grid=(sequences, groups), in_specs=[pl.Block...  9.55 us
    dot_general x1, matrix products, on_device(): jnp.dot(normed, branch_full, preferred_element_type=F32) * scales  9.32 us
  transfers between devices with their start and end apart: 3, of which 2 were waited for; matrix products, arithmetic and copies ran while one was open for 8% of the time, Pallas kernels for 55%

profile of v2, /device:TPU:0, one launch (start us, length us, event | category | flops | bytes accessed | tf_op | source)
XLA Modules:
  0.0 379.0 jit_solution(17023048875819067327)
XLA Ops:
  6.6 0.8 fusion.19
  7.3 0.7 subtract_convert_fusion
  8.1 1.3 multiply_convert_fusion.6
  9.4 0.9 pad_maximum_fusion
  10.4 0.9 maximum_maximum_fusion
  11.3 0.7 all-gather.4.cloned.1.call-update
  12.1 2.5 multiply_convert_fusion.2
  14.7 0.3 fusion.3
  15.0 1.2 fusion.4.x_ref
  16.2 32.4 %team_gather.2 = bf16[1024,2048]{1,0:T(8,128)(2,1)} custom-call(bf16[256,2048]{1,0:T(8,128)(2,1)} %fusion.4.x_ref), custom_call_target="tpu_custom_call" | custom-call | bytes 80000000 | tf_op jit(solution)/shard_map/team_gather/pallas_call | solution.py:137
  48.5 2.5 multiply_convert_fusion.3.x_ref
  51.0 103.3 %shard_gather.1 = bf16[2048,1536]{1,0:T(8,128)(2,1)} custom-call(bf16[256,1536]{1,0:T(8,128)(2,1)} %multiply_convert_fusion.3.x_ref), custom_call_target="tpu_custom_call" | custom-call | bytes 200000000 | tf_op jit(solution)/shard_map/shard_gather/pallas_call | solution.py:261
  155.0 0.7 fusion.14
  155.7 0.6 constant_dynamic-slice_fusion.2.taps_ref
  156.3 1.0 broadcast_select_fusion
  157.3 0.8 convert_add_fusion.2
  158.1 41.6 %all-gather.4.cloned.1.call-done = bf16[2048,1024]{1,0:T(8,128)(2,1)} async-done(((bf16[256,1024]{1,0:T(8,128)(2,1)}), bf16[2048,1024]{1,0:T(8,128)(2,1)}) %all-gather.4.cloned.1.call-update) | async-done | bytes 4194320 | tf_op jit(solution)/shard_map/all_gather | solution.py:302
  199.8 9.3 %multiply_convert_fusion.1.x_ref.gate_ref = bf16[1024,1024]{1,0:T(8,128)(2,1)} fusion(bf16[1024,2048]{1,0:T(8,128)(2,1)} %team_gather.2, bf16[2048,1024]{1,0:T(8,128)(2,1)} %all-gather.4.cloned.1.call-done, f32[1024]{0:T(1024)S(1)} %pad_maximum_fusion.1), kind=kOutput, calls=%fused_computation.1 | convolution fusion | flops 4297064448 | bytes 10489856 | tf_op jit(solution)/shard_map/dot_general | solution.py:320
  209.1 9.6 %mixer.1 = bf16[1024,512]{1,0:T(8,128)(2,1)} custom-call(bf16[1024,1024]{1,0:T(8,128)(2,1)} %multiply_convert_fusion.1.x_ref.gate_ref, bf16[1024,1024]{1,0:T(8,128)(2,1)} %multiply_convert_fusion.1.x_ref.gate_ref, f32[4,512]{1,0:T(4,128)} %constant_dynamic-slice_fusion.2.taps_ref, bf16[512,128]{1,0:T(8,128)(2,1)} %get-tuple-element.26.recur_ref, ...), custom_call_target="tpu_custom_call" | custom-call | flops 52428800 | bytes 3145728 | tf_op jit(solution)/shard_map/mixer/pallas_call | solution.py:55
  218.6 6.2 %convolution_convert_fusion.1.part_ref = bf16[1024,2048]{1,0:T(8,128)(2,1)} fusion(bf16[1024,512]{1,0:T(8,128)(2,1)} %mixer.1, bf16[528,2048]{1,0:T(8,128)(2,1)} %all-gather.6.cloned.1.call-done), kind=kOutput, calls=%fused_computation.3 | convolution fusion | flops 2149580800 | bytes 7340032 | tf_op jit(solution)/shard_map/dot_general | solution.py:335
  224.8 34.0 %team_sum.2 = f32[256,2048]{1,0:T(8,128)} custom-call(bf16[1024,2048]{1,0:T(8,128)(2,1)} %convolution_convert_fusion.1.part_ref), custom_call_target="tpu_custom_call" | custom-call | bytes 80000000 | tf_op jit(solution)/shard_map/team_sum/pallas_call | solution.py:207
  258.9 2.0 multiply_reduce_fusion.1
  260.9 0.3 copy-done.1
  261.2 0.6 fusion
  261.9 1.2 fusion.1.x_ref
  263.1 30.9 %team_gather.3 = bf16[1024,2048]{1,0:T(8,128)(2,1)} custom-call(bf16[256,2048]{1,0:T(8,128)(2,1)} %fusion.1.x_ref), custom_call_target="tpu_custom_call" | custom-call | bytes 80000000 | tf_op jit(solution)/shard_map/team_gather/pallas_call | solution.py:137
  293.9 21.2 %all-gather.8.cloned.1.call-done = bf16[1536,2048]{1,0:T(8,128)(2,1)} async-done(((bf16[1536,256]{1,0:T(8,128)(2,1)}), bf16[1536,2048]{1,0:T(8,128)(2,1)}) %all-gather.8.cloned.1.call-update) | async-done | bytes 6291472 | tf_op jit(solution)/shard_map/all_gather | solution.py:312
  315.1 19.9 %convolution_convert_fusion.part_ref = bf16[1024,2048]{1,0:T(8,128)(2,1)} fusion(bf16[1536,2048]{1,0:T(8,128)(2,1)} %all-gather.8.cloned.1.call-done, bf16[1024,2048]{1,0:T(8,128)(2,1)} %team_gather.3, bf16[2048,1536]{1,0:T(8,128)(2,1)} %shard_gather.1, f32[1536]{0:T(1024)S(1)} %dynamic_slice.50), kind=kOutput, calls=%fused_computation.2 | convolution fusion | flops 12893290496 | bytes 20977664 | tf_op jit(solution)/shard_map/dot_general | solution.py:340
  335.0 33.9 %team_sum.3 = f32[256,2048]{1,0:T(8,128)} custom-call(bf16[1024,2048]{1,0:T(8,128)(2,1)} %convolution_convert_fusion.part_ref), custom_call_target="tpu_custom_call" | custom-call | bytes 80000000 | tf_op jit(solution)/shard_map/team_sum/pallas_call | solution.py:207
  368.9 2.0 multiply_reduce_fusion
  370.9 0.2 copy-done.2
  371.1 1.3 fusion.7
  (53 shorter events, 0.9 us)
Async XLA Ops:
  6.5 149.1 %copy-start = (f32[4,1024]{1,0:T(4,128)S(1)}, f32[4,1024]{1,0:T(4,128)}, u32[]{:S(2)}) copy-start(f32[4,1024]{1,0:T(4,128)} %param.28) | copy-start | bytes 49156
  6.5 3.7 copy-start.4
  6.5 3.7 copy-start.8
  6.5 150.7 %all-gather.6.cloned.1.call-start = ((), (), s32[]{:S(2)}) async-start(), calls=%async_computation.1 | async-start | bytes 2433024 | tf_op jit(solution)/shard_map/all_gather | solution.py:311
  8.1 4.1 %copy-start.9 = (f32[256]{0:T(256)S(1)}, f32[256]{0:T(256)}, u32[]{:S(2)}) copy-start(f32[256]{0:T(256)} %param.37) | copy-start | bytes 3076
  10.4 4.2 %copy-start.3 = (bf16[1,512,2048]{2,1,0:T(8,128)(2,1)S(1)}, bf16[1,512,2048]{2,1,0:T(8,128)(2,1)}, u32[]{:S(2)}) copy-start(bf16[1,512,2048]{2,1,0:T(8,128)(2,1)} %param.19) | copy-start | bytes 6291460
  11.3 188.5 %all-gather.4.cloned.1.call-start = ((), (), s32[]{:S(2)}) async-start(), calls=%async_computation | async-start | bytes 4718592 | tf_op jit(solution)/shard_map/all_gather | solution.py:302
  12.1 303.1 %all-gather.8.cloned.1.call-start = ((), (), s32[]{:S(2)}) async-start(), calls=%async_computation.2 | async-start | bytes 7077888 | tf_op jit(solution)/shard_map/all_gather | solution.py:312
  16.2 32.4 %copy-start.10 = (f32[256]{0:T(256)S(1)}, f32[256]{0:T(256)}, u32[]{:S(2)}) copy-start(f32[256]{0:T(256)} %param.22) | copy-start | bytes 3076
  51.0 103.4 %copy-start.11 = (f32[1024]{0:T(1024)S(1)}, f32[1024]{0:T(1024)}, u32[]{:S(2)}) copy-start(f32[1024]{0:T(1024)} %param.26) | copy-start | bytes 12292
  51.0 103.5 %copy-start.12 = (f32[1024]{0:T(1024)S(1)}, f32[1024]{0:T(1024)}, u32[]{:S(2)}) copy-start(f32[1024]{0:T(1024)} %param.27) | copy-start | bytes 12292
  51.0 103.5 %copy-start.5 = (bf16[1024,32]{0,1:T(8,128)(2,1)S(1)}, bf16[1024,32]{0,1:T(8,128)(2,1)}, u32[]{:S(2)}) copy-start(bf16[1024,32]{0,1:T(8,128)(2,1)} %param.30) | copy-start | bytes 196612
  51.0 103.5 %copy-start.6 = (bf16[1024,32]{0,1:T(8,128)(2,1)S(1)}, bf16[1024,32]{0,1:T(8,128)(2,1)}, u32[]{:S(2)}) copy-start(bf16[1024,32]{0,1:T(8,128)(2,1)} %param.29) | copy-start | bytes 196612
  51.0 103.8 %copy-start.7 = (f32[3072]{0:T(1024)S(1)}, f32[3072]{0:T(1024)}, u32[]{:S(2)}) copy-start(f32[3072]{0:T(1024)} %param.35) | copy-start | bytes 36868
  51.0 103.9 %copy-start.13 = (f32[1024]{0:T(1024)S(1)}, f32[1024]{0:T(1024)}, u32[]{:S(2)}) copy-start(f32[1024]{0:T(1024)} %param.31) | copy-start | bytes 12292
  258.8 2.4 copy-start.1
  368.9 2.2 copy-start.2
Sparse Core Ops, SparseCore 0:
  11.4 89.6 all-gather.5
  103.3 96.4 all-gather.3
  201.8 113.2 all-gather.7
